TPU v7x, 32 devices: a whole 2x2x4 slice. The times are simulated.
32 devices in a mesh: ep: 16 (over z, y, x), tp: 2 (over core).
Axes of the slice: x: 2, y: 2, z: 4, core: 2. Of those that a mesh axis runs over, the one named last changes fastest.
Arguments:
- tokens: bfloat16 [1024, 2048], P('ep', 'tp'), may hold values from -6 to 6
- sequence_state_real: float32 [1024, 128, 64], P('ep', 'tp'), may hold values from -4 to 4
- sequence_state_imaginary: float32 [1024, 128, 64], P('ep', 'tp'), may hold values from -4 to 4
- mixer_norm_gain: float32 [2048], replicated, may hold values from 0.1 to 1.9
- expert_norm_gain: float32 [2048], replicated, may hold values from 0.1 to 1.9
- rate: float32 [128, 64], P('tp'), may hold values from 0.1 to 4
- freq: float32 [128, 64], P('tp'), may hold values from -3 to 3
- log_group_step: float32 [128], P('tp'), may hold values from -3 to 0
- input_map_real: float32 [128, 64, 16], P('tp'), may hold values from -1 to 1
- input_map_imaginary: float32 [128, 64, 16], P('tp'), may hold values from -1 to 1
- output_map_real: float32 [128, 16, 64], P('tp'), may hold values from -0.75 to 0.75
- output_map_imaginary: float32 [128, 16, 64], P('tp'), may hold values from -0.75 to 0.75
- skip: float32 [2048], P('tp'), may hold values from -4 to 4
- mixer_value_weight: bfloat16 [2048, 2048], P('tp'), may hold values from -0.125 to 0.125
- mixer_gate_weight: bfloat16 [2048, 2048], P('tp'), may hold values from -0.125 to 0.125
- group_router_weight: bfloat16 [2048, 4], replicated, may hold values from -0.125 to 0.125
- expert_router_weight: bfloat16 [2048, 16], replicated, may hold values from -0.125 to 0.125
- dense_blend_weight: float32 [2048], replicated, may hold values from -0.125 to 0.125
- routes: int32 [1024, 2], P('ep'), may hold values from 0 to 15, all different within a row; in each aligned block of 64 rows (0 to 63, 64 to 127, ...) at most 16 rows name the same one
- expert_gate_weight: bfloat16 [16, 2048, 1024], P('ep', None, 'tp'), may hold values from -0.125 to 0.125
- expert_up_weight: bfloat16 [16, 2048, 1024], P('ep', None, 'tp'), may hold values from -0.125 to 0.125
- expert_down_weight: bfloat16 [16, 1024, 2048], P('ep', 'tp'), may hold values from -0.1875 to 0.1875
- shared_gate_weight: bfloat16 [2048, 2048], P('tp', 'ep'), may hold values from -0.125 to 0.125
- shared_up_weight: bfloat16 [2048, 2048], P('tp', 'ep'), may hold values from -0.125 to 0.125
- shared_down_weight: bfloat16 [2048, 2048], P(None, 'tp'), may hold values from -0.125 to 0.125
Outputs:
- result: bfloat16 [1024, 2048], P('ep', 'tp')
- next_re: float32 [1024, 128, 64], P('ep', 'tp')
- next_im: float32 [1024, 128, 64], P('ep', 'tp')
Inputs may be any that keep to these rules, and one draw needn't show every extreme that they name: `routes`: each row names 2 different experts. Among the rows of one device no expert is named more than 16 times, and in every draw some expert is named exactly 16 times by some device's rows.
All inputs are finite; a program needn't handle non-finite values.
Results may differ from a plain program's by a relative error of at most 0.017.
Values may be sent and summed in bfloat16 or wider, within the bound.
A program may use at most 128 MiB of HBM per device.

v0:
```python
import jax
import jax.numpy as jnp
from jax import lax
from jax.sharding import PartitionSpec as P

NG = 4
EPS = 1e-06
PRECISION_MAX = lax.Precision.HIGHEST


def state_factors(rate, freq, log_group_step, input_map_real, input_map_imaginary):
    step_size = jnp.exp(log_group_step)[:, None]
    magnitude = jnp.exp(-rate * step_size)
    abar_re = magnitude * jnp.cos(freq * step_size)
    abar_im = magnitude * jnp.sin(freq * step_size)
    denom = rate * rate + freq * freq
    shift_re = abar_re - 1.0
    fac_re = (abar_im * freq - shift_re * rate) / denom
    fac_im = -(abar_im * rate + shift_re * freq) / denom
    bbar_re = fac_re[:, :, None] * input_map_real - fac_im[:, :, None] * input_map_imaginary
    bbar_im = fac_re[:, :, None] * input_map_imaginary + fac_im[:, :, None] * input_map_real
    return (abar_re, abar_im, bbar_re, bbar_im)


def state_step(
    normed,
    sequence_state_real,
    sequence_state_imaginary,
    factors,
    output_map_real,
    output_map_imaginary,
    skip,
):
    abar_re, abar_im, bbar_re, bbar_im = factors
    groups = abar_re.shape[0]
    inputs = normed.astype(jnp.float32)
    grouped = inputs.reshape(inputs.shape[0], groups, -1)
    drive_re = jnp.einsum("tgc,gpc->tgp", grouped, bbar_re, precision=PRECISION_MAX)
    drive_im = jnp.einsum("tgc,gpc->tgp", grouped, bbar_im, precision=PRECISION_MAX)
    fresh_real = abar_re * sequence_state_real - abar_im * sequence_state_imaginary + drive_re
    fresh_imaginary = abar_re * sequence_state_imaginary + abar_im * sequence_state_real + drive_im
    state_readout = jnp.einsum("dor,zdr->zdo", output_map_real, fresh_real, precision=PRECISION_MAX)
    state_readout = state_readout - jnp.einsum(
        "dor,zdr->zdo", output_map_imaginary, fresh_imaginary, precision=PRECISION_MAX
    )
    mixed = state_readout.reshape(inputs.shape) + skip * inputs
    return (mixed, fresh_real, fresh_imaginary)


def pair_product(left, first_map, second_map):
    first = jnp.dot(left, first_map, preferred_element_type=jnp.float32)
    second = jnp.dot(left, second_map, preferred_element_type=jnp.float32)
    return jnp.concatenate([first, second], axis=1)


def shards(
    tokens,
    sequence_state_real,
    sequence_state_imaginary,
    mixer_norm_gain,
    expert_norm_gain,
    rate,
    freq,
    log_group_step,
    input_map_real,
    input_map_imaginary,
    output_map_real,
    output_map_imaginary,
    skip,
    mixer_value_weight,
    mixer_gate_weight,
    group_router_weight,
    expert_router_weight,
    dense_blend_weight,
    routes,
    expert_gate_weight,
    expert_up_weight,
    expert_down_weight,
    shared_gate_weight,
    shared_up_weight,
    shared_down_weight,
):
    seq_rows, half_width = tokens.shape
    width = 2 * half_width
    column_start = lax.axis_index("tp") * half_width

    def own_rows(values):
        return lax.dynamic_slice_in_dim(values, column_start, half_width, 0)

    float_tokens = tokens.astype(jnp.float32)
    square_sum = lax.psum(jnp.sum(float_tokens * float_tokens, axis=1), "tp")
    first_scale = lax.rsqrt(square_sum / width + EPS)[:, None]
    normed = (float_tokens * first_scale * own_rows(mixer_norm_gain)).astype(jnp.bfloat16)
    factors = state_factors(rate, freq, log_group_step, input_map_real, input_map_imaginary)
    mixed, next_re, next_im = state_step(
        normed,
        sequence_state_real,
        sequence_state_imaginary,
        factors,
        output_map_real,
        output_map_imaginary,
        skip,
    )
    activated = jax.nn.gelu(mixed).astype(jnp.bfloat16)
    value_part = jnp.dot(activated, mixer_value_weight, preferred_element_type=jnp.float32)
    gate_part = jnp.dot(activated, mixer_gate_weight, preferred_element_type=jnp.float32)
    stacked = jnp.stack([value_part, gate_part], axis=1)
    mix_sum = lax.psum_scatter(
        stacked.astype(jnp.bfloat16), "tp", scatter_dimension=2, tiled=True
    ).astype(jnp.float32)
    mix_half = (mix_sum[:, 0] * jax.nn.sigmoid(mix_sum[:, 1])).astype(jnp.bfloat16)
    hidden = (float_tokens + mix_half.astype(jnp.float32)).astype(jnp.bfloat16)
    hidden_f32 = hidden.astype(jnp.float32)
    scaled = hidden_f32 * own_rows(expert_norm_gain)
    router_map = jnp.concatenate(
        [own_rows(group_router_weight), own_rows(expert_router_weight)], axis=1
    ).astype(jnp.float32)
    blend_map = own_rows(dense_blend_weight)
    hidden_squares = jnp.sum(hidden_f32 * hidden_f32, axis=1)
    total_squares = lax.psum(hidden_squares, "tp")
    inverse = lax.rsqrt(total_squares / width + EPS)[:, None]
    normal_rows = scaled * inverse
    raw_part = jnp.dot(normal_rows, router_map, precision=PRECISION_MAX)
    blend_part = jnp.dot(normal_rows, blend_map, precision=PRECISION_MAX)
    logits, blend_logit = lax.psum((raw_part, blend_part), "tp")
    hnorm = (scaled * inverse).astype(jnp.bfloat16)
    experts = expert_router_weight.shape[1]
    top_count = routes.shape[1]
    per_group = experts // NG
    group_prob = jax.nn.softmax(logits[:, :NG], axis=-1)
    expert_logits = logits[:, NG:]
    expert_hits = routes[:, :, None] == jnp.arange(experts, dtype=jnp.int32)[None, None, :]
    chosen = jnp.sum(jnp.where(expert_hits, expert_logits[:, None, :], 0.0), axis=2)
    group_hits = (routes // per_group)[:, :, None] == jnp.arange(NG, dtype=jnp.int32)[None, None, :]
    group_sel = jnp.sum(jnp.where(group_hits, group_prob[:, None, :], 0.0), axis=2)
    weights = jax.nn.softmax(chosen, axis=1) * group_sel
    full_rows = lax.all_gather(hnorm, "tp", axis=1, tiled=True)
    capacity = max(2, 2 * seq_rows * top_count // experts)
    flat_routes = routes.reshape(-1)
    matches = (flat_routes[:, None] == jnp.arange(experts, dtype=jnp.int32)[None, :]).astype(
        jnp.int32
    )
    slot_rank = jnp.sum(jnp.cumsum(matches, axis=0) * matches, axis=1) - 1
    slot_target = flat_routes * capacity + slot_rank
    dispatch = slot_target[None, :] == jnp.arange(experts * capacity, dtype=jnp.int32)[:, None]
    dispatch_rows = jnp.sum(
        dispatch.reshape(experts * capacity, seq_rows, top_count).astype(jnp.float32), axis=2
    )
    outgoing = jnp.dot(
        dispatch_rows.astype(jnp.bfloat16), full_rows, preferred_element_type=jnp.float32
    )
    outgoing = outgoing.astype(jnp.bfloat16).reshape(experts, capacity, width)
    received = lax.all_to_all(outgoing, "ep", split_axis=0, concat_axis=0, tiled=True)
    sources = received.shape[0]
    items = received.shape[1]
    token_rows = received.reshape(sources * items, width)
    gate_e = jnp.dot(token_rows, expert_gate_weight[0], preferred_element_type=jnp.float32)
    expert_up_rows = jnp.dot(token_rows, expert_up_weight[0], preferred_element_type=jnp.float32)
    inner = (jax.nn.silu(gate_e) * expert_up_rows).astype(jnp.bfloat16)
    part_out = jnp.dot(inner, expert_down_weight[0], preferred_element_type=jnp.float32)
    total = lax.psum_scatter(part_out.astype(jnp.bfloat16), "tp", scatter_dimension=1, tiled=True)
    finished = total.reshape(sources, items, half_width)
    returned = lax.all_to_all(finished, "ep", split_axis=0, concat_axis=0, tiled=True)
    returned_flat = returned.reshape(experts * capacity, half_width)
    picked = returned_flat[slot_target].reshape(seq_rows, top_count, half_width).astype(jnp.float32)
    routed = jnp.sum(weights[:, :, None] * picked, axis=1)
    partial_dense = pair_product(
        lax.all_gather(hnorm, "ep", axis=0, tiled=True), shared_gate_weight, shared_up_weight
    )
    dense_sum = lax.psum(partial_dense.astype(jnp.bfloat16), "tp").astype(jnp.float32)
    dense_cols = shared_gate_weight.shape[1]
    inner_cols = (jax.nn.silu(dense_sum[:, :dense_cols]) * dense_sum[:, dense_cols:]).astype(
        jnp.bfloat16
    )
    dense_inner = lax.all_to_all(inner_cols, "ep", split_axis=0, concat_axis=1, tiled=True)
    dense_out = jnp.dot(dense_inner, shared_down_weight, preferred_element_type=jnp.float32)
    result = hidden_f32 + routed + jax.nn.sigmoid(blend_logit)[:, None] * dense_out
    return (result.astype(jnp.bfloat16), next_re, next_im)


def solution(mesh):
    placed = (
        P("ep", "tp"),
        P("ep", "tp", None),
        P("ep", "tp", None),
        P(),
        P(),
        P("tp", None),
        P("tp", None),
        P("tp"),
        P("tp", None, None),
        P("tp", None, None),
        P("tp", None, None),
        P("tp", None, None),
        P("tp"),
        P("tp", None),
        P("tp", None),
        P(),
        P(),
        P(),
        P("ep", None),
        P("ep", None, "tp"),
        P("ep", None, "tp"),
        P("ep", "tp", None),
        P("tp", "ep"),
        P("tp", "ep"),
        P(None, "tp"),
    )
    return jax.shard_map(
        shards,
        mesh=mesh,
        in_specs=placed,
        out_specs=(P("ep", "tp"), P("ep", "tp", None), P("ep", "tp", None)),
        check_vma=False,
    )
```

profile of v0, /device:TPU:0, one launch (start us, length us, event | category | flops | bytes accessed | tf_op | source)
XLA Modules:
  0.0 187.7 jit_solution(3510667995029894204)
XLA Ops:
  7.2 3.5 %copy.64 = f32[64,64,64]{0,2,1:T(8,128)} copy(f32[64,64,64]{2,1,0:T(8,128)} %param.27) | data formatting | bytes 2097152 | tf_op args[2]
  10.7 3.4 %copy.63 = f32[64,64,64]{0,2,1:T(8,128)} copy(f32[64,64,64]{2,1,0:T(8,128)} %param.26) | data formatting | bytes 2097152 | tf_op args[1]
  14.3 2.6 %psum.35 = f32[64]{0:T(128)S(1)} all-reduce(f32[64]{0:T(128)S(1)} %fusion.29), channel_id=1, replica_groups=mesh['ep'=16,'tp'=2] {'tp'}, use_global_device_ids=true, to_apply=%region_1.0 | all-reduce | flops 64 | bytes 512 | tf_op jit(solution)/shard_map/psum | solution.py:91
  19.8 4.9 %bitcast_add_fusion.1 = f32[64,64,64]{0,2,1:T(8,128)S(1)} fusion(f32[64,64,64]{0,2,1:T(8,128)} %copy.64, f32[64,64,64]{0,2,1:T(8,128)} %copy.63, bf16[64,64,16]{0,2,1:T(8,128)(2,1)S(1)} %bitcast.75, f32[64,64]{1,0:T(8,128)S(1)} %get-tuple-element.17, f32[64,64]{1,0:T(8,128)S(1)} %get-tuple-element.18, f32[64,64,16]{1,2,0:T(8,128)S(1)} %copy-done.7, ...), kind=kOutput, calls=%fused_computation.13 | convolution fusion | flops 51576832 | bytes 3866624 | tf_op jit(solution)/shard_map/tgc,gpc->tgp/dot_general | solution.py:38
  24.8 3.2 %bitcast_add_fusion = f32[64,64,64]{0,2,1:T(8,128)S(1)} fusion(f32[64,64,64]{0,2,1:T(8,128)S(1)} %copy-done.4, f32[64,64,64]{0,2,1:T(8,128)S(1)} %copy-done.3, bf16[64,64,16]{0,2,1:T(8,128)(2,1)S(1)} %bitcast.76, f32[64,64]{1,0:T(8,128)S(1)} %get-tuple-element.17, f32[64,64]{1,0:T(8,128)S(1)} %get-tuple-element.18, f32[64,64,16]{1,2,0:T(8,128)S(1)} %copy-done.8, ...), kind=kOutput, calls=%fused_computation.12 | convolution fusion | flops 51576832 | bytes 3866624 | tf_op jit(solution)/shard_map/tgc,gpc->tgp/dot_general | solution.py:39
  30.0 1.9 %convolution_subtract_fusion = f32[64,64,16]{1,2,0:T(8,128)S(1)} fusion(f32[64,64,16]{1,2,0:T(8,128)S(1)} %fusion.77, f32[64,64,64]{0,2,1:T(8,128)S(1)} %bitcast_add_fusion, f32[64,16,64]{2,1,0:T(8,128)S(1)} %copy-done.10), kind=kOutput, calls=%fused_computation.15 | convolution fusion | flops 50397184 | bytes 1835008 | tf_op jit(solution)/shard_map/dor,zdr->zdo/dot_general | solution.py:43
  32.1 3.3 %fusion.1 = bf16[64,1,2048]{2,0,1:T(8,128)(2,1)S(1)} fusion(bf16[1024,2048]{1,0:T(8,128)(2,1)} %param.39, f32[64,1024]{1,0:T(8,128)S(1)} %copy.70, f32[1024]{0:T(1024)S(1)} %copy-done.14, f32[1024]{0:T(1024)S(1)} %dynamic_slice.15, f32[64]{0:T(128)S(1)} %add_rsqrt_fusion.1, bf16[64,1024]{1,0:T(8,128)(2,1)S(1)} %copy-done.6), kind=kOutput, calls=%fused_computation.6 | convolution fusion | flops 269615104 | bytes 4858112 | tf_op jit(solution)/shard_map/dot_general | solution.py:106
  37.8 10.3 %reduce-scatter.3.cloned.1.call-done = bf16[64,2,1024]{2,0,1:T(8,128)(2,1)} async-done(((bf16[64,2,2048]{2,0,1:T(8,128)(2,1)}), bf16[64,2,1024]{2,0,1:T(8,128)(2,1)}) %reduce-scatter.3.cloned.1.call-update) | async-done | bytes 262160 | tf_op jit(solution)/shard_map/reduce_scatter | solution.py:108
  49.3 2.5 %psum.36 = f32[64]{0:T(128)S(1)} all-reduce(f32[64]{0:T(128)S(1)} %get-tuple-element.14), channel_id=1, replica_groups=mesh['ep'=16,'tp'=2] {'tp'}, use_global_device_ids=true, to_apply=%region_4.0 | all-reduce | flops 64 | bytes 512 | tf_op jit(solution)/shard_map/psum | solution.py:120
  53.4 2.3 %all_gather.6 = bf16[64,2048]{1,0:T(8,128)(2,1)S(1)} all-gather(bf16[64,1024]{1,0:T(8,128)(2,1)} %fusion.43), channel_id=1, replica_groups=mesh['ep'=16,'tp'=2] {'tp'}, dimensions={1}, use_global_device_ids=true | all-gather | bytes 393216 | tf_op jit(solution)/shard_map/all_gather | solution.py:137
  56.2 41.0 %all_to_all.29 = bf16[16,16,2048]{2,1,0:T(8,128)(2,1)S(1)} all-to-all(bf16[16,16,2048]{2,1,0:T(8,128)(2,1)S(1)} %bitcast.74), channel_id=1, replica_groups=mesh['ep'=16,'tp'=2] {'ep'}, dimensions={0} | all-to-all | bytes 2097152 | tf_op jit(solution)/shard_map/all_to_all | solution.py:153
  98.9 4.2 %convolution_convert_fusion = bf16[256,2048]{1,0:T(8,128)(2,1)} fusion(bf16[1,512,2048]{2,1,0:T(8,128)(2,1)S(1)} %copy-done, bf16[256,2048]{1,0:T(8,128)(2,1)} %bitcast.79, bf16[1,2048,512]{2,1,0:T(8,128)(2,1)} %param.45, f32[256,512]{1,0:T(8,128)S(1)} %fusion.5), kind=kOutput, calls=%fused_computation.1 | convolution fusion | flops 1075052544 | bytes 6815744 | tf_op jit(solution)/shard_map/dot_general | solution.py:160
  103.1 3.8 %copy.77 = f32[64,64,64]{2,1,0:T(8,128)} copy(f32[64,64,64]{0,2,1:T(8,128)} %copy-done.2) | data formatting | bytes 2097152
  106.9 3.8 %copy.78 = f32[64,64,64]{2,1,0:T(8,128)} copy(f32[64,64,64]{0,2,1:T(8,128)} %copy-done.1) | data formatting | bytes 2097152
  111.7 3.3 %all-reduce = (f32[64,20]{0,1:T(8,128)S(1)}, f32[64]{0:T(128)S(1)}) all-reduce(f32[64,20]{0,1:T(8,128)S(1)} %fusion.44, f32[64]{0:T(128)S(1)} %convolution_bitcast_fusion), channel_id=1, replica_groups=mesh['ep'=16,'tp'=2] {'tp'}, use_global_device_ids=true, to_apply=%region_5.0 | all-reduce | flops 1344 | bytes 10752 | tf_op jit(solution)/shard_map/psum | solution.py:125
  115.1 3.4 %all-gather.2.cloned.1.call-done = bf16[1024,1024]{1,0:T(8,128)(2,1)} async-done(((bf16[64,1024]{1,0:T(8,128)(2,1)}), bf16[1024,1024]{1,0:T(8,128)(2,1)}) %all-gather.2.cloned.1.call-update) | async-done | bytes 2097168 | tf_op jit(solution)/shard_map/all_gather | solution.py:168
  118.5 2.4 %convolution_convert_fusion.4 = bf16[1024,128]{0,1:T(8,128)(2,1)S(1)} fusion(bf16[1024,1024]{1,0:T(8,128)(2,1)} %all-gather.2.cloned.1.call-done, bf16[1024,128]{1,0:T(8,128)(2,1)S(1)} %copy-done.12), kind=kOutput, calls=%fused_computation.17 | convolution fusion | flops 268566528 | bytes 2621440 | tf_op jit(solution)/shard_map/dot_general | solution.py:52
  120.9 7.1 %reduce-scatter.5.cloned.1.call-done = bf16[256,1024]{1,0:T(8,128)(2,1)} async-done(((bf16[256,2048]{1,0:T(8,128)(2,1)}), bf16[256,1024]{1,0:T(8,128)(2,1)}) %reduce-scatter.5.cloned.1.call-update) | async-done | bytes 524304 | tf_op jit(solution)/shard_map/reduce_scatter | solution.py:161
  128.0 6.8 %all-to-all-start.1 = ((bf16[16,16,1024]{2,1,0:T(8,128)(2,1)}), bf16[16,16,1024]{2,1,0:T(8,128)(2,1)S(1)}, u32[]{:S(2)}, u32[]{:S(2)}) async-start(bf16[16,16,1024]{2,1,0:T(8,128)(2,1)} %bitcast.80), calls=%async_computation.3 | async-start | bytes 1048576 | tf_op jit(solution)/shard_map/all_to_all | solution.py:163
  134.9 2.4 %convolution_convert_fusion.5 = bf16[1024,128]{0,1:T(8,128)(2,1)S(1)} fusion(bf16[1024,1024]{1,0:T(8,128)(2,1)} %all-gather.2.cloned.1.call-done, bf16[1024,128]{1,0:T(8,128)(2,1)S(1)} %copy-done.13), kind=kOutput, calls=%fused_computation.18 | convolution fusion | flops 268566528 | bytes 2621440 | tf_op jit(solution)/shard_map/dot_general | solution.py:51
  138.2 20.0 %all-reduce.3.cloned.1.call-done = bf16[1024,256]{0,1:T(8,128)(2,1)} async-done(((bf16[1024,256]{0,1:T(8,128)(2,1)}), bf16[1024,256]{0,1:T(8,128)(2,1)}) %all-reduce.3.cloned.1.call-update) | async-done | bytes 524304 | tf_op jit(solution)/shard_map/psum | solution.py:170
  160.3 6.8 %all-to-all-start.2 = ((bf16[16,64,128]{2,1,0:T(8,128)(2,1)}), bf16[16,64,128]{2,1,0:T(8,128)(2,1)S(1)}, u32[]{:S(2)}, u32[]{:S(2)}) async-start(bf16[16,64,128]{2,1,0:T(8,128)(2,1)} %bitcast.19), calls=%async_computation.4 | async-start | bytes 524288 | tf_op jit(solution)/shard_map/all_to_all | solution.py:175
  169.2 8.2 %all-to-all-done.2 = bf16[16,64,128]{2,1,0:T(8,128)(2,1)S(1)} async-done(((bf16[16,64,128]{2,1,0:T(8,128)(2,1)}), bf16[16,64,128]{2,1,0:T(8,128)(2,1)S(1)}, u32[]{:S(2)}, u32[]{:S(2)}) %all-to-all-start.2) | async-done | bytes 262176 | tf_op jit(solution)/shard_map/all_to_all | solution.py:175
  177.5 3.7 %fusion.14 = bf16[64,1024]{1,0:T(8,128)(2,1)} fusion(bf16[2048,1024]{1,0:T(8,128)(2,1)} %param.49, f32[64,1024]{1,0:T(8,128)S(1)} %multiply_reduce_fusion, bf16[64,1024]{1,0:T(8,128)(2,1)S(1)} %get-tuple-element.15, f32[64]{0:T(128)S(1)} %add_divide_fusion, bf16[16,64,128]{2,1,0:T(8,128)(2,1)S(1)} %all-to-all-done.2), kind=kOutput, calls=%fused_computation.21 | convolution fusion | flops 268763136 | bytes 4980992 | tf_op jit(solution)/shard_map/dot_general | solution.py:176
  (109 shorter events, 18.4 us)
Async XLA Ops:
  7.2 91.7 %copy-start = (bf16[1,512,2048]{2,1,0:T(8,128)(2,1)S(1)}, bf16[1,512,2048]{2,1,0:T(8,128)(2,1)}, u32[]{:S(2)}) copy-start(bf16[1,512,2048]{2,1,0:T(8,128)(2,1)} %param.46) | copy-start | bytes 6291460
  7.2 40.9 %reduce-scatter.3.cloned.1.call-start = ((), (), s32[]{:S(2)}) async-start(), calls=%async_computation.5 | async-start | bytes 786432 | tf_op jit(solution)/shard_map/reduce_scatter | solution.py:108
  10.7 3.4 %copy-start.6 = (bf16[64,1024]{1,0:T(8,128)(2,1)S(1)}, bf16[64,1024]{1,0:T(8,128)(2,1)}, u32[]{:S(2)}) copy-start(bf16[64,1024]{1,0:T(8,128)(2,1)} %param.25) | copy-start | bytes 393220
  10.7 6.2 %copy-start.18 = (f32[2048]{0:T(1024)S(1)}, f32[2048]{0:T(1024)}, u32[]{:S(2)}) copy-start(f32[2048]{0:T(1024)} %param.28) | copy-start | bytes 24580
  10.7 8.0 %copy-start.21 = (f32[64]{0:T(128)S(1)}, f32[64]{0:T(128)}, u32[]{:S(2)}) copy-start(f32[64]{0:T(128)} %param.32) | copy-start | bytes 772
  10.7 9.1 %copy-start.7 = (f32[64,64,16]{1,2,0:T(8,128)S(1)}, f32[64,64,16]{1,2,0:T(8,128)}, u32[]{:S(2)}) copy-start(f32[64,64,16]{1,2,0:T(8,128)} %param.34) | copy-start | bytes 786436
  10.7 9.1 %copy-start.8 = (f32[64,64,16]{1,2,0:T(8,128)S(1)}, f32[64,64,16]{1,2,0:T(8,128)}, u32[]{:S(2)}) copy-start(f32[64,64,16]{1,2,0:T(8,128)} %param.33) | copy-start | bytes 786436
  19.8 5.0 %copy-start.3 = (f32[64,64,64]{0,2,1:T(8,128)S(1)}, f32[64,64,64]{0,2,1:T(8,128)}, u32[]{:S(2)}) copy-start(f32[64,64,64]{0,2,1:T(8,128)} %copy.64) | copy-start | bytes 3145732
  19.8 5.0 %copy-start.4 = (f32[64,64,64]{0,2,1:T(8,128)S(1)}, f32[64,64,64]{0,2,1:T(8,128)}, u32[]{:S(2)}) copy-start(f32[64,64,64]{0,2,1:T(8,128)} %copy.63) | copy-start | bytes 3145732
  24.8 3.3 %copy-start.2 = (f32[64,64,64]{0,2,1:T(8,128)}, f32[64,64,64]{0,2,1:T(8,128)S(1)}, u32[]{:S(2)}) copy-start(f32[64,64,64]{0,2,1:T(8,128)S(1)} %bitcast_add_fusion.1) | copy-start | bytes 3145732
  24.8 3.3 %copy-start.11 = (f32[64,16,64]{2,1,0:T(8,128)S(1)}, f32[64,16,64]{2,1,0:T(8,128)}, u32[]{:S(2)}) copy-start(f32[64,16,64]{2,1,0:T(8,128)} %param.35) | copy-start | bytes 786436
  28.0 3.9 %copy-start.1 = (f32[64,64,64]{0,2,1:T(8,128)}, f32[64,64,64]{0,2,1:T(8,128)S(1)}, u32[]{:S(2)}) copy-start(f32[64,64,64]{0,2,1:T(8,128)S(1)} %bitcast_add_fusion) | copy-start | bytes 3145732
  32.1 3.5 %copy-start.5 = (bf16[1024,2048]{1,0:T(8,128)(2,1)S(1)}, bf16[1024,2048]{1,0:T(8,128)(2,1)}, u32[]{:S(2)}) copy-start(bf16[1024,2048]{1,0:T(8,128)(2,1)} %param.38) | copy-start | bytes 12582916
  37.4 81.1 %all-gather.2.cloned.1.call-start = ((), (), s32[]{:S(2)}) async-start(), calls=%async_computation.7 | async-start | bytes 2228224 | tf_op jit(solution)/shard_map/all_gather | solution.py:168
  52.5 75.5 %reduce-scatter.5.cloned.1.call-start = ((), (), s32[]{:S(2)}) async-start(), calls=%async_computation.6 | async-start | bytes 1572864 | tf_op jit(solution)/shard_map/reduce_scatter | solution.py:161
  53.3 44.9 %copy-start.20 = (bf16[1,2048,512]{2,1,0:T(8,128)(2,1)S(1)}, bf16[1,2048,512]{2,1,0:T(8,128)(2,1)}, u32[]{:S(2)}) copy-start(bf16[1,2048,512]{2,1,0:T(8,128)(2,1)} %param.44) | copy-start | bytes 6291460
  106.9 4.0 %copy-start.17 = (bf16[2048,4]{0,1:T(4,128)(2,1)S(1)}, bf16[2048,4]{0,1:T(4,128)(2,1)}, u32[]{:S(2)}) copy-start(bf16[2048,4]{0,1:T(4,128)(2,1)} %param.40) | copy-start | bytes 49156
  106.9 4.0 %copy-start.15 = (bf16[2048,16]{0,1:T(8,128)(2,1)S(1)}, bf16[2048,16]{0,1:T(8,128)(2,1)}, u32[]{:S(2)}) copy-start(bf16[2048,16]{0,1:T(8,128)(2,1)} %param.41) | copy-start | bytes 196612
  106.9 4.1 %dynamic-slice-start = ((f32[2048]{0:T(1024)}, s32[]{:T(128)}), f32[1024]{0:T(1024)S(1)}, s32[]{:S(2)}) async-start(f32[2048]{0:T(1024)} %param.42, s32[]{:T(128)} %select_n.30), calls=%async_computation.9 | async-start | bytes 8704 | tf_op jit(solution)/shard_map/dynamic_slice | solution.py:88
  106.9 11.6 %copy-start.12 = (bf16[1024,128]{1,0:T(8,128)(2,1)S(1)}, bf16[1024,128]{1,0:T(8,128)(2,1)}, u32[]{:S(2)}) copy-start(bf16[1024,128]{1,0:T(8,128)(2,1)} %param.48) | copy-start | bytes 786436
  111.0 23.9 %copy-start.13 = (bf16[1024,128]{1,0:T(8,128)(2,1)S(1)}, bf16[1024,128]{1,0:T(8,128)(2,1)}, u32[]{:S(2)}) copy-start(bf16[1024,128]{1,0:T(8,128)(2,1)} %param.47) | copy-start | bytes 786436
  128.0 32.3 %all-to-all-start.1 = ((bf16[16,16,1024]{2,1,0:T(8,128)(2,1)}), bf16[16,16,1024]{2,1,0:T(8,128)(2,1)S(1)}, u32[]{:S(2)}, u32[]{:S(2)}) async-start(bf16[16,16,1024]{2,1,0:T(8,128)(2,1)} %bitcast.80), calls=%async_computation.3 | async-start | bytes 1048576 | tf_op jit(solution)/shard_map/all_to_all | solution.py:163
  134.8 23.4 %all-reduce.3.cloned.1.call-start = ((), (), s32[]{:S(2)}) async-start(), calls=%async_computation.8 | async-start | bytes 1048576 | tf_op jit(solution)/shard_map/psum | solution.py:170
  160.3 17.1 %all-to-all-start.2 = ((bf16[16,64,128]{2,1,0:T(8,128)(2,1)}), bf16[16,64,128]{2,1,0:T(8,128)(2,1)S(1)}, u32[]{:S(2)}, u32[]{:S(2)}) async-start(bf16[16,64,128]{2,1,0:T(8,128)(2,1)} %bitcast.19), calls=%async_computation.4 | async-start | bytes 524288 | tf_op jit(solution)/shard_map/all_to_all | solution.py:175
  (5 other events, 8.9 us)
Sparse Core Ops, SparseCore 0:
  37.6 10.4 reduce-scatter.2
  52.6 65.8 all-gather.1
  120.8 7.2 reduce-scatter.4
  138.3 19.8 all-reduce.2
where the time goes:
time: 188 us
  blocking collectives  51.7 us (28%)
  waiting for transfers between devices  49.1 us (26%)
  matrix products  30.9 us (16%)
  local copies, waits for them, and re-layouts  19.7 us (10%)
  between operations  14.3 us (8%)
  starting transfers between devices  13.8 us (7%)
  other arithmetic  8.23 us (4%)
    all_to_all x1, blocking collectives, shards(): lax.all_to_all(outgoing, 'ep', split_axis=0, concat_axis=0, tiled=True)  41 us
    psum x1, waiting for transfers between devices, shards(): lax.psum(partial_dense.astype(jnp.bfloat16), 'tp').astype(jnp.float32)  20 us
    unnamed x49, local copies, waits for them, and re-layouts  15.8 us
    reduce_scatter x1, waiting for transfers between devices, shards(): lax.psum_scatter(stacked.astype(jnp.bfloat16), 'tp', scatter_dimension=2,...  10.3 us
    all_to_all x1, waiting for transfers between devices, shards(): lax.all_to_all(inner_cols, 'ep', split_axis=0, concat_axis=1, tiled=True)  8.24 us
    reduce_scatter x1, waiting for transfers between devices, shards(): lax.psum_scatter(part_out.astype(jnp.bfloat16), 'tp', scatter_dimension=1...  7.08 us
    all_to_all x1, starting transfers between devices, shards(): lax.all_to_all(inner_cols, 'ep', split_axis=0, concat_axis=1, tiled=True)  6.83 us
    all_to_all x1, starting transfers between devices, shards(): lax.all_to_all(finished, 'ep', split_axis=0, concat_axis=0, tiled=True)  6.79 us
  transfers between devices with their start and end apart: 6, of which 5 were waited for; matrix products, arithmetic and copies ran while one was open for 13% of the time, Pallas kernels for 0%

commit v1 on v0

--- a/solution.py
+++ b/solution.py
@@ -172,7 +172,10 @@
     inner_cols = (jax.nn.silu(dense_sum[:, :dense_cols]) * dense_sum[:, dense_cols:]).astype(
         jnp.bfloat16
     )
-    dense_inner = lax.all_to_all(inner_cols, "ep", split_axis=0, concat_axis=1, tiled=True)
+    dense_inner = jnp.concatenate(
+        lax.all_to_all(jnp.stack(jnp.split(inner_cols, lax.axis_size("ep"), axis=0)), "ep", 0, 0),
+        axis=1,
+    )
     dense_out = jnp.dot(dense_inner, shared_down_weight, preferred_element_type=jnp.float32)
     result = hidden_f32 + routed + jax.nn.sigmoid(blend_logit)[:, None] * dense_out
     return (result.astype(jnp.bfloat16), next_re, next_im)

time: 188 us -> 180 us (0.957)
  waiting for transfers between devices: 49.1 us -> 41 us
    psum x1, waiting for transfers between devices: 20 us -> 15.2 us  [shards(): lax.psum(partial_dense.astype(jnp.bfloat16), 'tp').astype(jnp.float32)]
    reduce_scatter x1, waiting for transfers between devices: 7.08 us -> 5.09 us  [shards(): lax.psum_scatter(part_out.astype(jnp.bfloat16), 'tp', scatter_dimension=1...]
    unnamed x49 -> x66, local copies, waits for them, and re-layouts: 15.8 us -> 16.6 us
  transfers between devices with their start and end apart: 6 -> 6, of which waited for: 5 -> 5; matrix products, arithmetic and copies ran while one was open for 13% -> 14% of each run, Pallas kernels for 0% -> 0%
where the time goes in v1:
time: 180 us
  blocking collectives  51.9 us (29%)
  waiting for transfers between devices  41 us (23%)
  matrix products  29.7 us (16%)
  local copies, waits for them, and re-layouts  20.7 us (12%)
  between operations  14.4 us (8%)
  starting transfers between devices  13.8 us (8%)
  other arithmetic  8.23 us (5%)
    all_to_all x1, blocking collectives, shards(): lax.all_to_all(outgoing, 'ep', split_axis=0, concat_axis=0, tiled=True)  41.1 us
    unnamed x66, local copies, waits for them, and re-layouts  16.6 us
    psum x1, waiting for transfers between devices, shards(): lax.psum(partial_dense.astype(jnp.bfloat16), 'tp').astype(jnp.float32)  15.2 us
    reduce_scatter x1, waiting for transfers between devices, shards(): lax.psum_scatter(stacked.astype(jnp.bfloat16), 'tp', scatter_dimension=2,...  10.3 us
    all_to_all x1, waiting for transfers between devices, shards(): lax.all_to_all(jnp.stack(jnp.split(inner_cols, lax.axis_size('ep'), axis=...  8.24 us
    all_to_all x1, starting transfers between devices, shards(): lax.all_to_all(jnp.stack(jnp.split(inner_cols, lax.axis_size('ep'), axis=...  6.83 us
    all_to_all x1, starting transfers between devices, shards(): lax.all_to_all(finished, 'ep', split_axis=0, concat_axis=0, tiled=True)  6.79 us
    reduce_scatter x1, waiting for transfers between devices, shards(): lax.psum_scatter(part_out.astype(jnp.bfloat16), 'tp', scatter_dimension=1...  5.09 us
  transfers between devices with their start and end apart: 6, of which 5 were waited for; matrix products, arithmetic and copies ran while one was open for 14% of the time, Pallas kernels for 0%

profile of v1, /device:TPU:0, one launch (start us, length us, event | category | flops | bytes accessed | tf_op | source)
XLA Modules:
  0.0 179.6 jit_solution(15755570435059114700)
XLA Ops:
  7.2 3.5 %copy.97 = f32[64,64,64]{0,2,1:T(8,128)} copy(f32[64,64,64]{2,1,0:T(8,128)} %param.27) | data formatting | bytes 2097152 | tf_op args[2]
  10.7 3.4 %copy.96 = f32[64,64,64]{0,2,1:T(8,128)} copy(f32[64,64,64]{2,1,0:T(8,128)} %param.26) | data formatting | bytes 2097152 | tf_op args[1]
  14.3 2.6 %psum.35 = f32[64]{0:T(128)S(1)} all-reduce(f32[64]{0:T(128)S(1)} %fusion.29), channel_id=1, replica_groups=mesh['ep'=16,'tp'=2] {'tp'}, use_global_device_ids=true, to_apply=%region_1.0 | all-reduce | flops 64 | bytes 512 | tf_op jit(solution)/shard_map/psum | solution.py:91
  19.8 4.9 %bitcast_add_fusion.1 = f32[64,64,64]{0,2,1:T(8,128)S(1)} fusion(f32[64,64,64]{0,2,1:T(8,128)} %copy.97, f32[64,64,64]{0,2,1:T(8,128)} %copy.96, bf16[64,64,16]{0,2,1:T(8,128)(2,1)S(1)} %bitcast.138, f32[64,64]{1,0:T(8,128)S(1)} %get-tuple-element.23, f32[64,64]{1,0:T(8,128)S(1)} %get-tuple-element.24, f32[64,64,16]{1,2,0:T(8,128)S(1)} %copy-done.8, ...), kind=kOutput, calls=%fused_computation.13 | convolution fusion | flops 51576832 | bytes 3866624 | tf_op jit(solution)/shard_map/tgc,gpc->tgp/dot_general | solution.py:38
  24.8 3.2 %bitcast_add_fusion = f32[64,64,64]{0,2,1:T(8,128)S(1)} fusion(f32[64,64,64]{0,2,1:T(8,128)S(1)} %copy-done.4, f32[64,64,64]{0,2,1:T(8,128)S(1)} %copy-done.3, bf16[64,64,16]{0,2,1:T(8,128)(2,1)S(1)} %bitcast.139, f32[64,64]{1,0:T(8,128)S(1)} %get-tuple-element.23, f32[64,64]{1,0:T(8,128)S(1)} %get-tuple-element.24, f32[64,64,16]{1,2,0:T(8,128)S(1)} %copy-done.9, ...), kind=kOutput, calls=%fused_computation.12 | convolution fusion | flops 51576832 | bytes 3866624 | tf_op jit(solution)/shard_map/tgc,gpc->tgp/dot_general | solution.py:39
  28.1 1.9 %fusion.93 = f32[64,64,16]{1,2,0:T(8,128)S(1)} fusion(f32[64,64,64]{0,2,1:T(8,128)S(1)} %bitcast_add_fusion.1, f32[64,16,64]{2,1,0:T(8,128)S(1)} %copy-done.12), kind=kOutput, calls=%fused_computation.155 | convolution fusion | flops 50331648 | bytes 1572864 | tf_op jit(solution)/shard_map/dor,zdr->zdo/dot_general | solution.py:42
  30.0 1.9 %convolution_subtract_fusion = f32[64,64,16]{1,2,0:T(8,128)S(1)} fusion(f32[64,64,16]{1,2,0:T(8,128)S(1)} %fusion.93, f32[64,64,64]{0,2,1:T(8,128)S(1)} %bitcast_add_fusion, f32[64,16,64]{2,1,0:T(8,128)S(1)} %copy-done.11), kind=kOutput, calls=%fused_computation.15 | convolution fusion | flops 50397184 | bytes 1835008 | tf_op jit(solution)/shard_map/dor,zdr->zdo/dot_general | solution.py:43
  32.1 3.3 %fusion.1 = bf16[64,1,2048]{2,0,1:T(8,128)(2,1)S(1)} fusion(bf16[1024,2048]{1,0:T(8,128)(2,1)} %param.39, f32[64,1024]{1,0:T(8,128)S(1)} %copy.103, f32[1024]{0:T(1024)S(1)} %copy-done.15, f32[1024]{0:T(1024)S(1)} %dynamic_slice.15, f32[64]{0:T(128)S(1)} %add_rsqrt_fusion.1, bf16[64,1024]{1,0:T(8,128)(2,1)S(1)} %copy-done.7), kind=kOutput, calls=%fused_computation.6 | convolution fusion | flops 269615104 | bytes 4858112 | tf_op jit(solution)/shard_map/dot_general | solution.py:106
  37.8 10.3 %reduce-scatter.3.cloned.1.call-done = bf16[64,2,1024]{2,0,1:T(8,128)(2,1)} async-done(((bf16[64,2,2048]{2,0,1:T(8,128)(2,1)}), bf16[64,2,1024]{2,0,1:T(8,128)(2,1)}) %reduce-scatter.3.cloned.1.call-update) | async-done | bytes 262160 | tf_op jit(solution)/shard_map/reduce_scatter | solution.py:108
  49.3 2.5 %psum.36 = f32[64]{0:T(128)S(1)} all-reduce(f32[64]{0:T(128)S(1)} %get-tuple-element.20), channel_id=1, replica_groups=mesh['ep'=16,'tp'=2] {'tp'}, use_global_device_ids=true, to_apply=%region_4.0 | all-reduce | flops 64 | bytes 512 | tf_op jit(solution)/shard_map/psum | solution.py:120
  53.4 2.3 %all_gather.6 = bf16[64,2048]{1,0:T(8,128)(2,1)S(1)} all-gather(bf16[64,1024]{1,0:T(8,128)(2,1)} %fusion.43), channel_id=1, replica_groups=mesh['ep'=16,'tp'=2] {'tp'}, dimensions={1}, use_global_device_ids=true | all-gather | bytes 393216 | tf_op jit(solution)/shard_map/all_gather | solution.py:137
  56.2 41.1 %all_to_all.15 = bf16[16,16,2048]{2,1,0:T(8,128)(2,1)S(1)} all-to-all(bf16[16,16,2048]{2,1,0:T(8,128)(2,1)S(1)} %bitcast.137), channel_id=1, replica_groups=mesh['ep'=16,'tp'=2] {'ep'}, dimensions={0} | all-to-all | bytes 2097152 | tf_op jit(solution)/shard_map/all_to_all | solution.py:153
  99.0 4.5 %convolution_convert_fusion = bf16[256,2048]{1,0:T(8,128)(2,1)} fusion(bf16[1,512,2048]{2,1,0:T(8,128)(2,1)S(1)} %copy-done, bf16[256,2048]{1,0:T(8,128)(2,1)} %bitcast.142, bf16[1,2048,512]{2,1,0:T(8,128)(2,1)} %param.45, f32[256,512]{1,0:T(8,128)S(1)} %fusion.5), kind=kOutput, calls=%fused_computation.1 | convolution fusion | flops 1075052544 | bytes 6815744 | tf_op jit(solution)/shard_map/dot_general | solution.py:160
  103.6 3.8 %copy.110 = f32[64,64,64]{2,1,0:T(8,128)} copy(f32[64,64,64]{0,2,1:T(8,128)} %copy-done.2) | data formatting | bytes 2097152
  107.4 3.8 %copy.111 = f32[64,64,64]{2,1,0:T(8,128)} copy(f32[64,64,64]{0,2,1:T(8,128)} %copy-done.1) | data formatting | bytes 2097152
  112.2 3.3 %all-reduce = (f32[64,20]{0,1:T(8,128)S(1)}, f32[64]{0:T(128)S(1)}) all-reduce(f32[64,20]{0,1:T(8,128)S(1)} %fusion.44, f32[64]{0:T(128)S(1)} %convolution_bitcast_fusion), channel_id=1, replica_groups=mesh['ep'=16,'tp'=2] {'tp'}, use_global_device_ids=true, to_apply=%region_5.0 | all-reduce | flops 1344 | bytes 10752 | tf_op jit(solution)/shard_map/psum | solution.py:125
  115.5 2.1 %all-gather.2.cloned.1.call-done = bf16[1024,1024]{1,0:T(8,128)(2,1)} async-done(((bf16[64,1024]{1,0:T(8,128)(2,1)}), bf16[1024,1024]{1,0:T(8,128)(2,1)}) %all-gather.2.cloned.1.call-update) | async-done | bytes 2097168 | tf_op jit(solution)/shard_map/all_gather | solution.py:168
  117.6 2.6 %convolution_convert_fusion.4 = bf16[1024,128]{0,1:T(8,128)(2,1)S(1)} fusion(bf16[1024,1024]{1,0:T(8,128)(2,1)} %all-gather.2.cloned.1.call-done, bf16[1024,128]{1,0:T(8,128)(2,1)S(1)} %copy-done.13), kind=kOutput, calls=%fused_computation.17 | convolution fusion | flops 268566528 | bytes 2621440 | tf_op jit(solution)/shard_map/dot_general | solution.py:52
  122.0 5.1 %reduce-scatter.5.cloned.1.call-done = bf16[256,1024]{1,0:T(8,128)(2,1)} async-done(((bf16[256,2048]{1,0:T(8,128)(2,1)}), bf16[256,1024]{1,0:T(8,128)(2,1)}) %reduce-scatter.5.cloned.1.call-update) | async-done | bytes 524304 | tf_op jit(solution)/shard_map/reduce_scatter | solution.py:161
  127.1 6.8 %all-to-all-start.1 = ((bf16[16,16,1024]{2,1,0:T(8,128)(2,1)}), bf16[16,16,1024]{2,1,0:T(8,128)(2,1)S(1)}, u32[]{:S(2)}, u32[]{:S(2)}) async-start(bf16[16,16,1024]{2,1,0:T(8,128)(2,1)} %bitcast.143), calls=%async_computation.3 | async-start | bytes 1048576 | tf_op jit(solution)/shard_map/all_to_all | solution.py:163
  133.9 15.2 %all-reduce.3.cloned.1.call-done = bf16[1024,256]{0,1:T(8,128)(2,1)} async-done(((bf16[1024,256]{0,1:T(8,128)(2,1)}), bf16[1024,256]{0,1:T(8,128)(2,1)}) %all-reduce.3.cloned.1.call-update) | async-done | bytes 524304 | tf_op jit(solution)/shard_map/psum | solution.py:170
  152.3 6.8 %all-to-all-start.2 = ((bf16[16,64,128]{2,1,0:T(8,128)(2,1)}), bf16[16,64,128]{2,1,0:T(8,128)(2,1)S(1)}, u32[]{:S(2)}, u32[]{:S(2)}) async-start(bf16[16,64,128]{2,1,0:T(8,128)(2,1)} %copy.108), calls=%async_computation.4 | async-start | bytes 524288 | tf_op jit(solution)/shard_map/all_to_all | solution.py:176
  161.2 8.2 %all-to-all-done.2 = bf16[16,64,128]{2,1,0:T(8,128)(2,1)S(1)} async-done(((bf16[16,64,128]{2,1,0:T(8,128)(2,1)}), bf16[16,64,128]{2,1,0:T(8,128)(2,1)S(1)}, u32[]{:S(2)}, u32[]{:S(2)}) %all-to-all-start.2) | async-done | bytes 262176 | tf_op jit(solution)/shard_map/all_to_all | solution.py:176
  169.4 3.7 %fusion.14 = bf16[64,1024]{1,0:T(8,128)(2,1)} fusion(bf16[2048,1024]{1,0:T(8,128)(2,1)} %param.49, f32[64,1024]{1,0:T(8,128)S(1)} %multiply_reduce_fusion, bf16[64,1024]{1,0:T(8,128)(2,1)S(1)} %get-tuple-element.21, f32[64]{0:T(128)S(1)} %add_divide_fusion, bf16[16,64,128]{2,1,0:T(8,128)(2,1)S(1)} %all-to-all-done.2), kind=kOutput, calls=%fused_computation.21 | convolution fusion | flops 268763136 | bytes 4980992 | tf_op jit(solution)/shard_map/dot_general | solution.py:179
  (127 shorter events, 18.3 us)
Async XLA Ops:
  7.2 91.8 %copy-start = (bf16[1,512,2048]{2,1,0:T(8,128)(2,1)S(1)}, bf16[1,512,2048]{2,1,0:T(8,128)(2,1)}, u32[]{:S(2)}) copy-start(bf16[1,512,2048]{2,1,0:T(8,128)(2,1)} %param.46) | copy-start | bytes 6291460
  7.2 40.9 %reduce-scatter.3.cloned.1.call-start = ((), (), s32[]{:S(2)}) async-start(), calls=%async_computation.5 | async-start | bytes 786432 | tf_op jit(solution)/shard_map/reduce_scatter | solution.py:108
  10.7 3.4 %copy-start.7 = (bf16[64,1024]{1,0:T(8,128)(2,1)S(1)}, bf16[64,1024]{1,0:T(8,128)(2,1)}, u32[]{:S(2)}) copy-start(bf16[64,1024]{1,0:T(8,128)(2,1)} %param.25) | copy-start | bytes 393220
  10.7 6.2 %copy-start.19 = (f32[2048]{0:T(1024)S(1)}, f32[2048]{0:T(1024)}, u32[]{:S(2)}) copy-start(f32[2048]{0:T(1024)} %param.28) | copy-start | bytes 24580
  10.7 8.0 %copy-start.22 = (f32[64]{0:T(128)S(1)}, f32[64]{0:T(128)}, u32[]{:S(2)}) copy-start(f32[64]{0:T(128)} %param.32) | copy-start | bytes 772
  10.7 9.1 %copy-start.8 = (f32[64,64,16]{1,2,0:T(8,128)S(1)}, f32[64,64,16]{1,2,0:T(8,128)}, u32[]{:S(2)}) copy-start(f32[64,64,16]{1,2,0:T(8,128)} %param.34) | copy-start | bytes 786436
  10.7 9.1 %copy-start.9 = (f32[64,64,16]{1,2,0:T(8,128)S(1)}, f32[64,64,16]{1,2,0:T(8,128)}, u32[]{:S(2)}) copy-start(f32[64,64,16]{1,2,0:T(8,128)} %param.33) | copy-start | bytes 786436
  19.8 5.0 %copy-start.3 = (f32[64,64,64]{0,2,1:T(8,128)S(1)}, f32[64,64,64]{0,2,1:T(8,128)}, u32[]{:S(2)}) copy-start(f32[64,64,64]{0,2,1:T(8,128)} %copy.97) | copy-start | bytes 3145732
  19.8 5.0 %copy-start.4 = (f32[64,64,64]{0,2,1:T(8,128)S(1)}, f32[64,64,64]{0,2,1:T(8,128)}, u32[]{:S(2)}) copy-start(f32[64,64,64]{0,2,1:T(8,128)} %copy.96) | copy-start | bytes 3145732
  24.8 3.3 %copy-start.2 = (f32[64,64,64]{0,2,1:T(8,128)}, f32[64,64,64]{0,2,1:T(8,128)S(1)}, u32[]{:S(2)}) copy-start(f32[64,64,64]{0,2,1:T(8,128)S(1)} %bitcast_add_fusion.1) | copy-start | bytes 3145732
  24.8 3.3 %copy-start.12 = (f32[64,16,64]{2,1,0:T(8,128)S(1)}, f32[64,16,64]{2,1,0:T(8,128)}, u32[]{:S(2)}) copy-start(f32[64,16,64]{2,1,0:T(8,128)} %param.35) | copy-start | bytes 786436
  28.0 3.9 %copy-start.1 = (f32[64,64,64]{0,2,1:T(8,128)}, f32[64,64,64]{0,2,1:T(8,128)S(1)}, u32[]{:S(2)}) copy-start(f32[64,64,64]{0,2,1:T(8,128)S(1)} %bitcast_add_fusion) | copy-start | bytes 3145732
  32.1 3.5 %copy-start.6 = (bf16[1024,2048]{1,0:T(8,128)(2,1)S(1)}, bf16[1024,2048]{1,0:T(8,128)(2,1)}, u32[]{:S(2)}) copy-start(bf16[1024,2048]{1,0:T(8,128)(2,1)} %param.38) | copy-start | bytes 12582916
  37.4 80.2 %all-gather.2.cloned.1.call-start = ((), (), s32[]{:S(2)}) async-start(), calls=%async_computation.7 | async-start | bytes 2228224 | tf_op jit(solution)/shard_map/all_gather | solution.py:168
  52.5 74.6 %reduce-scatter.5.cloned.1.call-start = ((), (), s32[]{:S(2)}) async-start(), calls=%async_computation.6 | async-start | bytes 1572864 | tf_op jit(solution)/shard_map/reduce_scatter | solution.py:161
  53.3 45.0 %copy-start.21 = (bf16[1,2048,512]{2,1,0:T(8,128)(2,1)S(1)}, bf16[1,2048,512]{2,1,0:T(8,128)(2,1)}, u32[]{:S(2)}) copy-start(bf16[1,2048,512]{2,1,0:T(8,128)(2,1)} %param.44) | copy-start | bytes 6291460
  103.5 45.6 %all-reduce.3.cloned.1.call-start = ((), (), s32[]{:S(2)}) async-start(), calls=%async_computation.8 | async-start | bytes 1048576 | tf_op jit(solution)/shard_map/psum | solution.py:170
  107.4 4.0 %copy-start.18 = (bf16[2048,4]{0,1:T(4,128)(2,1)S(1)}, bf16[2048,4]{0,1:T(4,128)(2,1)}, u32[]{:S(2)}) copy-start(bf16[2048,4]{0,1:T(4,128)(2,1)} %param.40) | copy-start | bytes 49156
  107.4 4.0 %copy-start.16 = (bf16[2048,16]{0,1:T(8,128)(2,1)S(1)}, bf16[2048,16]{0,1:T(8,128)(2,1)}, u32[]{:S(2)}) copy-start(bf16[2048,16]{0,1:T(8,128)(2,1)} %param.41) | copy-start | bytes 196612
  107.4 4.1 %dynamic-slice-start = ((f32[2048]{0:T(1024)}, s32[]{:T(128)}), f32[1024]{0:T(1024)S(1)}, s32[]{:S(2)}) async-start(f32[2048]{0:T(1024)} %param.42, s32[]{:T(128)} %select_n.30), calls=%async_computation.9 | async-start | bytes 8704 | tf_op jit(solution)/shard_map/dynamic_slice | solution.py:88
  107.4 10.3 %copy-start.13 = (bf16[1024,128]{1,0:T(8,128)(2,1)S(1)}, bf16[1024,128]{1,0:T(8,128)(2,1)}, u32[]{:S(2)}) copy-start(bf16[1024,128]{1,0:T(8,128)(2,1)} %param.48) | copy-start | bytes 786436
  111.2 9.0 %copy-start.14 = (bf16[1024,128]{1,0:T(8,128)(2,1)S(1)}, bf16[1024,128]{1,0:T(8,128)(2,1)}, u32[]{:S(2)}) copy-start(bf16[1024,128]{1,0:T(8,128)(2,1)} %param.47) | copy-start | bytes 786436
  127.1 25.2 %all-to-all-start.1 = ((bf16[16,16,1024]{2,1,0:T(8,128)(2,1)}), bf16[16,16,1024]{2,1,0:T(8,128)(2,1)S(1)}, u32[]{:S(2)}, u32[]{:S(2)}) async-start(bf16[16,16,1024]{2,1,0:T(8,128)(2,1)} %bitcast.143), calls=%async_computation.3 | async-start | bytes 1048576 | tf_op jit(solution)/shard_map/all_to_all | solution.py:163
  152.3 17.1 %all-to-all-start.2 = ((bf16[16,64,128]{2,1,0:T(8,128)(2,1)}), bf16[16,64,128]{2,1,0:T(8,128)(2,1)S(1)}, u32[]{:S(2)}, u32[]{:S(2)}) async-start(bf16[16,64,128]{2,1,0:T(8,128)(2,1)} %copy.108), calls=%async_computation.4 | async-start | bytes 524288 | tf_op jit(solution)/shard_map/all_to_all | solution.py:176
  (6 other events, 11.5 us)
Sparse Core Ops, SparseCore 0:
  37.6 10.4 reduce-scatter.2
  52.6 64.9 all-gather.1
  119.9 7.1 reduce-scatter.4
  129.3 19.7 all-reduce.2
